TPU v7x, 32 devices: a whole 2x2x4 slice. The times are simulated.
32 devices in a mesh: grp: 2 (over y), ep: 8 (over z, core), tp: 2 (over x).
Axes of the slice: x: 2, y: 2, z: 4, core: 2. Of those that a mesh axis runs over, the one named last changes fastest.
Arguments:
- resid_in: bfloat16 [176, 2048], P(('grp', 'ep')), parts along dimension 0, may hold values from -6 to 6
- norm_attn: float32 [2048], replicated, may hold values from 0.1 to 1.9
- norm_moe: float32 [2048], replicated, may hold values from 0.1 to 1.9
- w_query: bfloat16 [2048, 1024], P('ep', 'tp'), may hold values from -0.125 to 0.125
- w_key: bfloat16 [2048, 256], P('ep', 'tp'), may hold values from -0.125 to 0.125
- w_value: bfloat16 [2048, 256], P('ep', 'tp'), may hold values from -0.125 to 0.125
- head_offset: float32 [16], P('tp'), may hold values from 1.5 to 9.5
- kv_cache: bfloat16 [176, 1024, 4, 128], P(('grp', 'ep'), None, 'tp'), parts along dimension 0, may hold values from -6 to 6
- lengths: int32 [176], P(('grp', 'ep')), parts along dimension 0, may hold values from 128 to 1024, as said below
- w_output: bfloat16 [1024, 2048], P('tp', 'ep'), may hold values from -0.375 to 0.375
- routes: int32 [176, 4], P(('grp', 'ep')), parts along dimension 0, may hold values from 0 to 7, all different within a row; in each aligned block of 11 rows (0 to 10, 11 to 21, ...) at most 7 rows name the same one
- route_weights: float32 [176, 4], P(('grp', 'ep')), parts along dimension 0, may hold values from 0.2 to 1
- gate_experts: bfloat16 [8, 2048, 512], P('ep', None, 'tp'), may hold values from -0.125 to 0.125
- up_experts: bfloat16 [8, 2048, 512], P('ep', None, 'tp'), may hold values from -0.125 to 0.125
- down_experts: bfloat16 [8, 512, 2048], P('ep', 'tp'), may hold values from -0.25 to 0.25
- gate_shared: bfloat16 [2048, 512], P('ep', 'tp'), may hold values from -0.125 to 0.125
- up_shared: bfloat16 [2048, 512], P('ep', 'tp'), may hold values from -0.125 to 0.125
- down_shared: bfloat16 [512, 2048], P('tp', 'ep'), may hold values from -0.25 to 0.25
Outputs:
- layer_out: bfloat16 [176, 2048], P(('grp', 'ep'), 'tp'), parts along dimension 0
- new_rows: bfloat16 [176, 4, 128], P(('grp', 'ep'), 'tp'), parts along dimension 0
There are 2 independent parts, one for each index of `grp`. A program takes and returns all parts, laid end to end along the dimension named above; an argument that names none is the same for every part. Nothing has to cross between parts.
Inputs may be any that keep to these rules, and one draw needn't show every extreme that they name: `routes`: among the rows of one device no expert is named more than 7 times, and in every draw some expert is named exactly 7 times by one device's rows; a row names 4 different experts. Sequence b's new token follows cache positions 0 to lengths[b] - 1; the other positions are not read.
All inputs are finite; a program needn't handle non-finite values.
Results may differ from a plain program's by a relative error of at most 0.015.
Values may be sent and summed in bfloat16 or wider, within the bound.
No kernel may reach another device: no remote copies, remote signals or barrier semaphores. Data moves between devices by JAX's collectives and lax.ppermute only.
A program may use at most 64 MiB of HBM per device.

v0:
```python
import jax
import jax.numpy as jnp
from jax import lax
from jax.sharding import PartitionSpec as P

HEAD = 64
TOPK = 4
EPS = 1e-06


def rms_scale(row_block, gain):
    rows_wide = row_block.astype(jnp.float32)
    inverse = lax.rsqrt(jnp.mean(rows_wide * rows_wide, axis=-1, keepdims=True) + EPS)
    return rows_wide * inverse * gain


def stick_read(query, kv_cache, lengths, offsets):
    seq_count = query.shape[0]
    kv_local = kv_cache.shape[2]
    head_local = offsets.shape[0]
    per_group = head_local // kv_local
    cache_len = kv_cache.shape[1]
    grouped = query.reshape(seq_count, kv_local, per_group, HEAD)
    key_rows = kv_cache[:, :, :, :HEAD]
    value_rows = kv_cache[:, :, :, HEAD:]
    scores = jnp.einsum("skgd,slkd->skgl", grouped, key_rows, preferred_element_type=jnp.float32)
    scores = scores * HEAD ** (-0.5) - offsets.reshape(1, kv_local, per_group, 1)
    positions = lax.broadcasted_iota(jnp.int32, (seq_count, cache_len), 1)
    alive_mask = (positions < lengths[:, None])[:, None, None, :]
    remain = jnp.where(alive_mask, jax.nn.log_sigmoid(-scores), 0.0)
    suffix = lax.cumsum(remain, axis=3, reverse=True) - remain
    stick = jnp.where(alive_mask, jnp.exp(jax.nn.log_sigmoid(scores) + suffix), 0.0).astype(
        jnp.bfloat16
    )
    mixed_out = jnp.einsum("skgl,slkd->skgd", stick, value_rows, preferred_element_type=jnp.float32)
    return mixed_out.reshape(seq_count, head_local * HEAD).astype(jnp.bfloat16)


def on_device(
    resid_in,
    norm_attn,
    norm_moe,
    w_query,
    w_key,
    w_value,
    head_offset,
    kv_cache,
    lengths,
    w_output,
    routes,
    route_weights,
    gate_experts,
    up_experts,
    down_experts,
    gate_shared,
    up_shared,
    down_shared,
):
    tok_count = resid_in.shape[0]
    n_ep = lax.axis_size("ep")
    normed = rms_scale(resid_in, norm_attn).astype(jnp.bfloat16)
    k_cols = w_key.shape[1]
    pieces = (
        lax.all_gather(w_query, "ep", axis=0, tiled=True),
        lax.all_gather(w_key, "ep", axis=0, tiled=True),
        lax.all_gather(w_value, "ep", axis=0, tiled=True),
    )
    sliced = normed
    query_f, key_f, value_f = tuple(
        (
            jnp.dot(sliced, weight_piece, preferred_element_type=jnp.float32)
            for weight_piece in pieces
        )
    )
    query = query_f.astype(jnp.bfloat16)
    kv_local = k_cols // HEAD
    key_new = key_f.astype(jnp.bfloat16).reshape(tok_count, kv_local, HEAD)
    value_new = value_f.astype(jnp.bfloat16).reshape(tok_count, kv_local, HEAD)
    new_rows = jnp.concatenate([key_new, value_new], axis=2)
    attended = stick_read(query, kv_cache, lengths, head_offset)
    attn_part = jnp.dot(
        attended,
        lax.all_gather(w_output, "ep", axis=1, tiled=True),
        preferred_element_type=jnp.float32,
    ).astype(jnp.bfloat16)
    attn_sum = lax.psum(attn_part, "tp").astype(jnp.float32)
    resid_mid = (resid_in.astype(jnp.float32) + attn_sum).astype(jnp.bfloat16)
    normed_moe = rms_scale(resid_mid, norm_moe).astype(jnp.bfloat16)
    pieces = (
        lax.all_gather(gate_shared, "ep", axis=0, tiled=True),
        lax.all_gather(up_shared, "ep", axis=0, tiled=True),
    )
    sliced = normed_moe
    gate_s = jnp.dot(sliced, pieces[0], preferred_element_type=jnp.float32)
    up_s = jnp.dot(sliced, pieces[1], preferred_element_type=jnp.float32)
    hidden_shared = (jax.nn.silu(gate_s) * up_s).astype(jnp.bfloat16)
    shared_part = jnp.dot(
        hidden_shared,
        lax.all_gather(down_shared, "ep", axis=1, tiled=True),
        preferred_element_type=jnp.float32,
    ).astype(jnp.bfloat16)
    shared_out = lax.psum_scatter(shared_part, "tp", scatter_dimension=1, tiled=True).astype(
        jnp.float32
    )
    local_experts = gate_experts.shape[0]
    experts_all = local_experts * n_ep
    capacity = min(tok_count, tok_count * TOPK // experts_all + 2)
    flat_routes = routes.reshape(-1)
    expert_ids = lax.broadcasted_iota(jnp.int32, (1, experts_all), 1)
    onehot = (flat_routes[:, None] == expert_ids).astype(jnp.int32)
    slots = jnp.sum((jnp.cumsum(onehot, axis=0) - onehot) * onehot, axis=1)
    expert_grid = lax.broadcasted_iota(jnp.int32, (experts_all, capacity, 1), 0)
    slot_grid = lax.broadcasted_iota(jnp.int32, (experts_all, capacity, 1), 1)
    match = (
        (flat_routes[None, None, :] == expert_grid) & (slots[None, None, :] == slot_grid)
    ).astype(jnp.bfloat16)
    source_rows = jnp.repeat(normed_moe, TOPK, axis=0)
    outgoing = jnp.einsum(
        "ecr,rd->ecd", match, source_rows, preferred_element_type=jnp.float32
    ).astype(jnp.bfloat16)
    arrived = lax.all_to_all(outgoing, "ep", split_axis=0, concat_axis=0, tiled=True)
    slot_count = arrived.shape[1]
    grouped_in = arrived.reshape(n_ep, local_experts, slot_count, arrived.shape[2])
    gate_h = jnp.einsum(
        "secd,edf->secf", grouped_in, gate_experts, preferred_element_type=jnp.float32
    )
    up_h = jnp.einsum("secd,edf->secf", grouped_in, up_experts, preferred_element_type=jnp.float32)
    hidden_e = (jax.nn.silu(gate_h) * up_h).astype(jnp.bfloat16)
    down_h = jnp.einsum(
        "secf,efd->secd", hidden_e, down_experts, preferred_element_type=jnp.float32
    ).astype(jnp.bfloat16)
    summed = (
        lax.psum_scatter(down_h, "tp", scatter_dimension=3, tiled=True)
        .astype(jnp.float32)
        .astype(jnp.bfloat16)
    )
    summed = summed.reshape(n_ep * local_experts, slot_count, summed.shape[3])
    returned = lax.all_to_all(summed, "ep", split_axis=0, concat_axis=0, tiled=True)
    gathered_back = jnp.einsum("ecr,ecd->rd", match, returned, preferred_element_type=jnp.float32)
    col_width = gathered_back.shape[1]
    weighted = gathered_back.reshape(tok_count, TOPK, col_width) * route_weights[:, :, None]
    routed = jnp.sum(weighted, axis=1)
    own_cols = lax.dynamic_slice_in_dim(resid_mid, lax.axis_index("tp") * col_width, col_width, 1)
    layer_out = (own_cols.astype(jnp.float32) + shared_out + routed).astype(jnp.bfloat16)
    return (layer_out, new_rows)


def solution(mesh):
    return jax.shard_map(
        on_device,
        mesh=mesh,
        in_specs=(
            P(("grp", "ep"), None),
            P(),
            P(),
            P("ep", "tp"),
            P("ep", "tp"),
            P("ep", "tp"),
            P("tp"),
            P(("grp", "ep"), None, "tp", None),
            P(("grp", "ep")),
            P("tp", "ep"),
            P(("grp", "ep"), None),
            P(("grp", "ep"), None),
            P("ep", None, "tp"),
            P("ep", None, "tp"),
            P("ep", "tp", None),
            P("ep", "tp"),
            P("ep", "tp"),
            P("tp", "ep"),
        ),
        out_specs=(P(("grp", "ep"), "tp"), P(("grp", "ep"), "tp", None)),
        check_vma=False,
    )
```

profile of v0, /device:TPU:0, one launch (start us, length us, event | category | flops | bytes accessed | tf_op | source)
XLA Modules:
  0.0 270.2 jit_solution(16846753004733863255)
XLA Ops:
  7.2 0.7 all-gather.6.cloned.1.call-update
  8.0 0.7 all-gather.8.cloned.1.call-update
  8.7 0.7 all-gather.10.cloned.1.call-update
  9.4 1.0 fusion.33
  10.5 12.9 %fusion.66 = (bf16[11,1024,2,64]{3,2,1,0:T(2,128)(2,1)}, bf16[11,1024,2,64]{3,2,1,0:T(2,128)(2,1)}) fusion(bf16[11,1024,2,128]{3,2,1,0:T(2,128)(2,1)} %param.25), kind=kLoop, calls=%fused_computation.81 | loop fusion | bytes 11534336 | tf_op jit(solution)/shard_map/slice | solution.py:24
  24.1 17.4 %all-gather.6.cloned.1.call-done = bf16[2048,512]{1,0:T(8,128)(2,1)} async-done(((bf16[256,512]{1,0:T(8,128)(2,1)}), bf16[2048,512]{1,0:T(8,128)(2,1)}) %all-gather.6.cloned.1.call-update) | async-done | bytes 2097168 | tf_op jit(solution)/shard_map/all_gather | solution.py:64
  41.5 2.0 convolution_convert_fusion.4
  43.6 4.3 %fusion.26 = (f32[11,2,4,1024]{3,2,1,0:T(4,128)S(1)}, f32[11,2,4,1024]{3,2,1,0:T(4,128)S(1)}) fusion(pred[11,1024]{1,0:T(8,128)(4,1)S(1)} %iota_compare_fusion, f32[2,4]{1,0:T(2,128)S(1)} %sub.16, bf16[11,2,4,64]{3,2,1,0:T(4,128)(2,1)S(1)} %reshape.94, bf16[11,1024,2,64]{3,2,1,0:T(2,128)(2,1)} %get-tuple-element.4), kind=kOutput, calls=%fused_computation.31 | convolution fusion | flops 12435456 | bytes 3627040 | tf_op jit(solution)/shard_map/skgd,slkd->skgl/dot_general | solution.py:26
  48.0 108.9 %reduce-window.6 = f32[11,2,4,8,128]{4,3,2,1,0:T(8,128)S(1)} reduce-window(f32[11,2,4,8,128]{4,3,2,1,0:T(8,128)S(1)} %reshape.95, f32[]{:T(128)} %constant.15.clone.1), window={size=1x1x1x1x128 pad=0_0x0_0x0_0x0_0x0_127}, to_apply=%region_1.2 | reduce-window | flops 11444224 | bytes 720900 | tf_op jit(solution)/shard_map/reduce-window
  157.0 0.5 copy.31
  158.0 4.4 %fusion.11 = bf16[11,2,4,64]{3,2,1,0:T(4,128)(2,1)S(1)} fusion(bf16[11,1024,2,64]{3,2,1,0:T(2,128)(2,1)} %get-tuple-element.5, f32[11,2,4,1024]{3,2,1,0:T(4,128)S(1)} %reduce_window_sum.26, f32[11,2,4,1024]{3,2,1,0:T(4,128)S(1)} %get-tuple-element.7, pred[11,1024]{1,0:T(8,128)(4,1)S(1)} %iota_compare_fusion), kind=kOutput, calls=%fused_computation.12 | convolution fusion | flops 13342208 | bytes 3627008 | tf_op jit(solution)/shard_map/skgl,slkd->skgd/dot_general | solution.py:35
  162.5 2.0 convolution_convert_fusion.3
  164.5 8.8 %psum.7 = bf16[11,2048]{1,0:T(8,128)(2,1)S(1)} all-reduce(bf16[11,2048]{1,0:T(8,128)(2,1)S(1)} %convolution_convert_fusion.3), channel_id=1, replica_groups=mesh['grp'=2,'ep'=8,'tp'=2] {'tp'}, use_global_device_ids=true, to_apply=%region_3.4 | all-reduce | flops 22528 | bytes 90112 | tf_op jit(solution)/shard_map/psum | solution.py:86
  174.0 12.6 %all_to_all.10 = bf16[8,7,2048]{2,1,0:T(8,128)(2,1)S(1)} all-to-all(bf16[8,7,2048]{2,1,0:T(8,128)(2,1)S(1)} %copy.35), channel_id=1, replica_groups=mesh['grp'=2,'ep'=8,'tp'=2] {'ep'}, dimensions={0} | all-to-all | bytes 458752 | tf_op jit(solution)/shard_map/all_to_all | solution.py:121
  186.6 0.3 fusion.16
  187.0 1.6 fusion.18
  188.5 1.0 fusion.4
  189.6 0.5 all-gather.12.cloned.1.call-update
  190.2 0.5 all-gather.14.cloned.1.call-update
  190.8 14.9 %all_gather.26 = bf16[2048,128]{1,0:T(8,128)(2,1)S(1)} all-gather(bf16[256,128]{1,0:T(8,128)(2,1)S(1)} %copy-done.4), channel_id=1, replica_groups=mesh['grp'=2,'ep'=8,'tp'=2] {'ep'}, dimensions={0}, use_global_device_ids=true | all-gather | bytes 589824 | tf_op jit(solution)/shard_map/all_gather | solution.py:65
  205.8 0.2 convolution_convert_fusion.6
  206.1 16.9 %all_gather.27 = bf16[2048,128]{1,0:T(8,128)(2,1)S(1)} all-gather(bf16[256,128]{1,0:T(8,128)(2,1)S(1)} %copy-done.5), channel_id=1, replica_groups=mesh['grp'=2,'ep'=8,'tp'=2] {'ep'}, dimensions={0}, use_global_device_ids=true | all-gather | bytes 589824 | tf_op jit(solution)/shard_map/all_gather | solution.py:66
  223.0 0.2 convolution_convert_fusion.5
  223.3 0.7 pad_maximum_fusion
  224.0 1.5 fusion.67
  225.5 1.6 copy.38
  227.1 3.4 %all-to-all-start.1 = ((bf16[8,7,1024]{2,1,0:T(8,128)(2,1)}), bf16[8,7,1024]{2,1,0:T(8,128)(2,1)S(1)}, u32[]{:S(2)}, u32[]{:S(2)}) async-start(bf16[8,7,1024]{2,1,0:T(8,128)(2,1)} %copy.38), calls=%async_computation.3 | async-start | bytes 262144 | tf_op jit(solution)/shard_map/all_to_all | solution.py:138
  230.5 19.6 %all-gather.14.cloned.1.call-done = bf16[256,2048]{1,0:T(8,128)(2,1)} async-done(((bf16[256,256]{1,0:T(8,128)(2,1)}), bf16[256,2048]{1,0:T(8,128)(2,1)}) %all-gather.14.cloned.1.call-update) | async-done | bytes 1048592 | tf_op jit(solution)/shard_map/all_gather | solution.py:99
  250.1 2.9 %convolution_convert_fusion.2 = bf16[11,2048]{1,0:T(8,128)(2,1)} fusion(bf16[256,2048]{1,0:T(8,128)(2,1)} %all-gather.14.cloned.1.call-done, bf16[11,2048]{1,0:T(8,128)(2,1)S(1)} %fusion.32, bf16[2048,256]{1,0:T(8,128)(2,1)} %all-gather.12.cloned.1.call-done, f32[11,256]{1,0:T(8,128)S(1)} %fusion.67), kind=kOutput, calls=%fused_computation.7 | convolution fusion | flops 23108096 | bytes 2198528 | tf_op jit(solution)/shard_map/dot_general | solution.py:97
  253.1 0.2 convolution_bitcast_fusion
  253.5 8.5 %reduce-scatter.3.cloned.1.call-done = bf16[11,1024]{1,0:T(8,128)(2,1)} async-done(((bf16[11,2048]{1,0:T(8,128)(2,1)}), bf16[11,1024]{1,0:T(8,128)(2,1)}) %reduce-scatter.3.cloned.1.call-update) | async-done | bytes 22544 | tf_op jit(solution)/shard_map/reduce_scatter | solution.py:102
  262.0 1.4 add_convert_fusion
  (64 shorter events, 3.1 us)
Async XLA Ops:
  7.2 181.4 %copy-start = (bf16[1,256,2048]{2,1,0:T(8,128)(2,1)S(1)}, bf16[1,256,2048]{2,1,0:T(8,128)(2,1)}, u32[]{:S(2)}) copy-start(bf16[1,256,2048]{2,1,0:T(8,128)(2,1)} %param.32) | copy-start | bytes 3145732
  7.2 34.3 %all-gather.6.cloned.1.call-start = ((), (), s32[]{:S(2)}) async-start(), calls=%async_computation.4 | async-start | bytes 2359296 | tf_op jit(solution)/shard_map/all_gather | solution.py:64
  7.9 154.6 %all-gather.8.cloned.1.call-start = ((), (), s32[]{:S(2)}) async-start(), calls=%async_computation.5 | async-start | bytes 2359296 | tf_op jit(solution)/shard_map/all_gather | solution.py:83
  8.7 215.3 %all-gather.10.cloned.1.call-start = ((), (), s32[]{:S(2)}) async-start(), calls=%async_computation.6 | async-start | bytes 1179648 | tf_op jit(solution)/shard_map/all_gather | solution.py:90
  9.4 216.1 %reduce-scatter.5.cloned.1.call-start = ((), (), s32[]{:S(2)}) async-start(), calls=%async_computation.10 | async-start | bytes 344064 | tf_op jit(solution)/shard_map/reduce_scatter | solution.py:133
  10.4 13.0 %copy-start.9 = (s32[11]{0:T(128)S(1)}, s32[11]{0:T(128)}, u32[]{:S(2)}) copy-start(s32[11]{0:T(128)} %param.26) | copy-start | bytes 136
  10.4 13.1 %copy-start.10 = (f32[8]{0:T(128)S(1)}, f32[8]{0:T(128)}, u32[]{:S(2)}) copy-start(f32[8]{0:T(128)} %param.24) | copy-start | bytes 100
  10.4 13.2 %copy-start.7 = (s32[11,4]{0,1:T(4,128)S(1)}, s32[11,4]{0,1:T(4,128)}, u32[]{:S(2)}) copy-start(s32[11,4]{0,1:T(4,128)} %param.28) | copy-start | bytes 532
  10.5 31.0 %copy-start.1 = (bf16[11,2048]{1,0:T(8,128)(2,1)S(1)}, bf16[11,2048]{1,0:T(8,128)(2,1)}, u32[]{:S(2)}) copy-start(bf16[11,2048]{1,0:T(8,128)(2,1)} %param.18) | copy-start | bytes 135172
  10.5 31.0 %copy-start.3 = (f32[2048]{0:T(1024)S(1)}, f32[2048]{0:T(1024)}, u32[]{:S(2)}) copy-start(f32[2048]{0:T(1024)} %param.19) | copy-start | bytes 24580
  158.0 15.5 %copy-start.6 = (f32[2048]{0:T(1024)S(1)}, f32[2048]{0:T(1024)}, u32[]{:S(2)}) copy-start(f32[2048]{0:T(1024)} %param.20) | copy-start | bytes 24580
  158.0 28.6 %copy-start.2 = (bf16[1,2048,256]{2,1,0:T(8,128)(2,1)S(1)}, bf16[1,2048,256]{2,1,0:T(8,128)(2,1)}, u32[]{:S(2)}) copy-start(bf16[1,2048,256]{2,1,0:T(8,128)(2,1)} %param.31) | copy-start | bytes 3145732
  162.4 28.4 %copy-start.8 = (f32[11,4]{0,1:T(4,128)S(1)}, f32[11,4]{0,1:T(4,128)}, u32[]{:S(2)}) copy-start(f32[11,4]{0,1:T(4,128)} %param.29) | copy-start | bytes 532
  162.4 28.5 %copy-start.4 = (bf16[256,128]{1,0:T(8,128)(2,1)S(1)}, bf16[256,128]{1,0:T(8,128)(2,1)}, u32[]{:S(2)}) copy-start(bf16[256,128]{1,0:T(8,128)(2,1)} %param.22) | copy-start | bytes 196612
  162.4 43.7 %copy-start.5 = (bf16[256,128]{1,0:T(8,128)(2,1)S(1)}, bf16[256,128]{1,0:T(8,128)(2,1)}, u32[]{:S(2)}) copy-start(bf16[256,128]{1,0:T(8,128)(2,1)} %param.23) | copy-start | bytes 196612
  189.6 41.0 %all-gather.12.cloned.1.call-start = ((), (), s32[]{:S(2)}) async-start(), calls=%async_computation.7 | async-start | bytes 1179648 | tf_op jit(solution)/shard_map/all_gather | solution.py:91
  190.2 60.0 %all-gather.14.cloned.1.call-start = ((), (), s32[]{:S(2)}) async-start(), calls=%async_computation.8 | async-start | bytes 1179648 | tf_op jit(solution)/shard_map/all_gather | solution.py:99
  227.1 26.0 %all-to-all-start.1 = ((bf16[8,7,1024]{2,1,0:T(8,128)(2,1)}), bf16[8,7,1024]{2,1,0:T(8,128)(2,1)S(1)}, u32[]{:S(2)}, u32[]{:S(2)}) async-start(bf16[8,7,1024]{2,1,0:T(8,128)(2,1)} %copy.38), calls=%async_computation.3 | async-start | bytes 262144 | tf_op jit(solution)/shard_map/all_to_all | solution.py:138
  230.5 31.5 %reduce-scatter.3.cloned.1.call-start = ((), (), s32[]{:S(2)}) async-start(), calls=%async_computation.9 | async-start | bytes 98304 | tf_op jit(solution)/shard_map/reduce_scatter | solution.py:102
Sparse Core Ops, SparseCore 0:
  9.6 31.8 all-gather.5
  43.1 30.0 all-gather.7
  74.8 21.2 all-gather.9
  189.7 9.3 reduce-scatter.4
  200.5 24.5 all-gather.11
  226.6 23.5 all-gather.13
  253.2 8.7 reduce-scatter.2
where the time goes:
time: 271 us; the launch traced here: 270 us
  other arithmetic  113 us (42%)
  blocking collectives  53.2 us (20%)
  waiting for transfers between devices  48.6 us (18%)
  matrix products  20.8 us (8%)
  local copies, waits for them, and re-layouts  16.5 us (6%)
  between operations  14.4 us (5%)
  starting transfers between devices  3.64 us (1%)
    another operation x2, other arithmetic  109 us
    all_gather x1, waiting for transfers between devices, on_device(): lax.all_gather(down_shared, 'ep', axis=1, tiled=True)  19.6 us
    all_gather x1, waiting for transfers between devices, on_device(): lax.all_gather(w_query, 'ep', axis=0, tiled=True)  17.4 us
    all_gather x1, blocking collectives, on_device(): lax.all_gather(w_value, 'ep', axis=0, tiled=True)  16.9 us
    all_gather x1, blocking collectives, on_device(): lax.all_gather(w_key, 'ep', axis=0, tiled=True)  14.9 us
    slice x1, local copies, waits for them, and re-layouts, stick_read(): key_rows = kv_cache[:, :, :, :HEAD]  12.9 us
    all_to_all x1, blocking collectives, on_device(): lax.all_to_all(outgoing, 'ep', split_axis=0, concat_axis=0, tiled=True)  12.6 us
    psum x1, blocking collectives, on_device(): attn_sum = lax.psum(attn_part, 'tp').astype(jnp.float32)  8.79 us
  transfers between devices with their start and end apart: 8, of which 3 were waited for; matrix products, arithmetic and copies ran while one was open for 55% of the time, Pallas kernels for 0%

commit v1 on v0

--- a/solution.py
+++ b/solution.py
@@ -94,9 +94,12 @@
     gate_s = jnp.dot(sliced, pieces[0], preferred_element_type=jnp.float32)
     up_s = jnp.dot(sliced, pieces[1], preferred_element_type=jnp.float32)
     hidden_shared = (jax.nn.silu(gate_s) * up_s).astype(jnp.bfloat16)
+    report_the_levels_all = lambda field, axis_key: jnp.concatenate(
+        lax.all_gather(field, axis_name=axis_key), axis=1
+    )
     shared_part = jnp.dot(
         hidden_shared,
-        lax.all_gather(down_shared, "ep", axis=1, tiled=True),
+        report_the_levels_all(down_shared, axis_key="ep"),
         preferred_element_type=jnp.float32,
     ).astype(jnp.bfloat16)
     shared_out = lax.psum_scatter(shared_part, "tp", scatter_dimension=1, tiled=True).astype(

time: 271 us -> 254 us (0.937)
  waiting for transfers between devices: 48.6 us -> 30.2 us
    all_gather x1, waiting for transfers between devices: 19.6 us -> 0.01 us  [on_device(): lax.all_gather(field, axis_name=axis_key)]
    all_to_all x1, waiting for transfers between devices: 0.01 us -> 3.9 us  [on_device(): lax.all_to_all(summed, 'ep', split_axis=0, concat_axis=0, tiled=True)]
  transfers between devices with their start and end apart: 8 -> 8, of which waited for: 3 -> 3; matrix products, arithmetic and copies ran while one was open for 55% -> 60% of each run, Pallas kernels for 0% -> 0%
where the time goes in v1:
time: 254 us
  other arithmetic  113 us (44%)
  blocking collectives  52.9 us (21%)
  waiting for transfers between devices  30.2 us (12%)
  matrix products  21.4 us (8%)
  local copies, waits for them, and re-layouts  18 us (7%)
  between operations  14.4 us (6%)
  starting transfers between devices  3.64 us (1%)
    another operation x2, other arithmetic  109 us
    all_gather x1, waiting for transfers between devices, on_device(): lax.all_gather(w_query, 'ep', axis=0, tiled=True)  16.8 us
    all_gather x1, blocking collectives, on_device(): lax.all_gather(w_value, 'ep', axis=0, tiled=True)  16.6 us
    all_gather x1, blocking collectives, on_device(): lax.all_gather(w_key, 'ep', axis=0, tiled=True)  14.9 us
    slice x1, local copies, waits for them, and re-layouts, stick_read(): key_rows = kv_cache[:, :, :, :HEAD]  12.9 us
    all_to_all x1, blocking collectives, on_device(): lax.all_to_all(outgoing, 'ep', split_axis=0, concat_axis=0, tiled=True)  12.6 us
    psum x1, blocking collectives, on_device(): attn_sum = lax.psum(attn_part, 'tp').astype(jnp.float32)  8.79 us
    reduce_scatter x1, waiting for transfers between devices, on_device(): lax.psum_scatter(shared_part, 'tp', scatter_dimension=1, tiled=True)  6.32 us
  transfers between devices with their start and end apart: 8, of which 3 were waited for; matrix products, arithmetic and copies ran while one was open for 60% of the time, Pallas kernels for 0%

profile of v1, /device:TPU:0, one launch (start us, length us, event | category | flops | bytes accessed | tf_op | source)
XLA Modules:
  0.0 253.6 jit_solution(12424076745943716333)
XLA Ops:
  7.2 0.7 all-gather.7.cloned.1.call-update
  8.0 0.7 all-gather.9.cloned.1.call-update
  8.7 0.7 all-gather.15.cloned.1.call-update
  9.4 0.5 all-gather.11.cloned.1.call-update
  10.0 1.0 fusion.33
  11.1 12.9 %fusion.66 = (bf16[11,1024,2,64]{3,2,1,0:T(2,128)(2,1)}, bf16[11,1024,2,64]{3,2,1,0:T(2,128)(2,1)}) fusion(bf16[11,1024,2,128]{3,2,1,0:T(2,128)(2,1)} %param.25), kind=kLoop, calls=%fused_computation.81 | loop fusion | bytes 11534336 | tf_op jit(solution)/shard_map/slice | solution.py:24
  24.7 16.8 %all-gather.7.cloned.1.call-done = bf16[2048,512]{1,0:T(8,128)(2,1)} async-done(((bf16[256,512]{1,0:T(8,128)(2,1)}), bf16[2048,512]{1,0:T(8,128)(2,1)}) %all-gather.7.cloned.1.call-update) | async-done | bytes 2097168 | tf_op jit(solution)/shard_map/all_gather | solution.py:64
  41.5 2.0 convolution_convert_fusion.4
  43.6 5.0 %fusion.26 = (f32[11,2,4,1024]{3,2,1,0:T(4,128)S(1)}, f32[11,2,4,1024]{3,2,1,0:T(4,128)}) fusion(pred[11,1024]{1,0:T(8,128)(4,1)S(1)} %iota_compare_fusion, f32[2,4]{1,0:T(2,128)S(1)} %sub.16, bf16[11,2,4,64]{3,2,1,0:T(4,128)(2,1)S(1)} %reshape.100, bf16[11,1024,2,64]{3,2,1,0:T(2,128)(2,1)} %get-tuple-element.4), kind=kOutput, calls=%fused_computation.31 | convolution fusion | flops 12435456 | bytes 3627040 | tf_op jit(solution)/shard_map/skgd,slkd->skgl/dot_general | solution.py:26
  48.7 108.9 %reduce-window.6 = f32[11,2,4,8,128]{4,3,2,1,0:T(8,128)S(1)} reduce-window(f32[11,2,4,8,128]{4,3,2,1,0:T(8,128)S(1)} %reshape.101, f32[]{:T(128)} %constant.15.clone.1), window={size=1x1x1x1x128 pad=0_0x0_0x0_0x0_0x0_127}, to_apply=%region_1.2 | reduce-window | flops 11444224 | bytes 720900 | tf_op jit(solution)/shard_map/reduce-window
  157.7 0.5 copy.38
  158.7 4.5 %fusion.11 = bf16[11,2,4,64]{3,2,1,0:T(4,128)(2,1)S(1)} fusion(bf16[11,1024,2,64]{3,2,1,0:T(2,128)(2,1)} %get-tuple-element.5, f32[11,2,4,1024]{3,2,1,0:T(4,128)S(1)} %reduce_window_sum.26, f32[11,2,4,1024]{3,2,1,0:T(4,128)} %get-tuple-element.7, pred[11,1024]{1,0:T(8,128)(4,1)S(1)} %iota_compare_fusion), kind=kOutput, calls=%fused_computation.12 | convolution fusion | flops 13342208 | bytes 3627008 | tf_op jit(solution)/shard_map/skgl,slkd->skgd/dot_general | solution.py:35
  163.3 2.0 convolution_convert_fusion.3
  165.3 8.8 %psum.7 = bf16[11,2048]{1,0:T(8,128)(2,1)S(1)} all-reduce(bf16[11,2048]{1,0:T(8,128)(2,1)S(1)} %convolution_convert_fusion.3), channel_id=1, replica_groups=mesh['grp'=2,'ep'=8,'tp'=2] {'tp'}, use_global_device_ids=true, to_apply=%region_3.4 | all-reduce | flops 22528 | bytes 90112 | tf_op jit(solution)/shard_map/psum | solution.py:86
  174.8 12.6 %all_to_all.10 = bf16[8,7,2048]{2,1,0:T(8,128)(2,1)S(1)} all-to-all(bf16[8,7,2048]{2,1,0:T(8,128)(2,1)S(1)} %copy.43), channel_id=1, replica_groups=mesh['grp'=2,'ep'=8,'tp'=2] {'ep'}, dimensions={0} | all-to-all | bytes 458752 | tf_op jit(solution)/shard_map/all_to_all | solution.py:124
  187.4 0.3 fusion.16
  187.8 1.6 fusion.18
  189.3 1.0 fusion.4
  190.4 0.5 all-gather.13.cloned.1.call-update
  191.1 14.9 %all_gather.30 = bf16[2048,128]{1,0:T(8,128)(2,1)S(1)} all-gather(bf16[256,128]{1,0:T(8,128)(2,1)S(1)} %copy-done.4), channel_id=1, replica_groups=mesh['grp'=2,'ep'=8,'tp'=2] {'ep'}, dimensions={0}, use_global_device_ids=true | all-gather | bytes 589824 | tf_op jit(solution)/shard_map/all_gather | solution.py:65
  206.0 0.2 convolution_convert_fusion.6
  206.3 16.6 %all_gather.31 = bf16[2048,128]{1,0:T(8,128)(2,1)S(1)} all-gather(bf16[256,128]{1,0:T(8,128)(2,1)S(1)} %copy-done.5), channel_id=1, replica_groups=mesh['grp'=2,'ep'=8,'tp'=2] {'ep'}, dimensions={0}, use_global_device_ids=true | all-gather | bytes 589824 | tf_op jit(solution)/shard_map/all_gather | solution.py:66
  222.9 0.2 convolution_convert_fusion.5
  223.2 0.7 pad_maximum_fusion
  223.9 1.5 copy.41
  225.4 1.5 fusion.67
  226.9 1.6 copy.46
  228.5 3.4 %all-to-all-start.1 = ((bf16[8,7,1024]{2,1,0:T(8,128)(2,1)}), bf16[8,7,1024]{2,1,0:T(8,128)(2,1)S(1)}, u32[]{:S(2)}, u32[]{:S(2)}) async-start(bf16[8,7,1024]{2,1,0:T(8,128)(2,1)} %copy.46), calls=%async_computation.3 | async-start | bytes 262144 | tf_op jit(solution)/shard_map/all_to_all | solution.py:141
  232.0 2.7 %convolution_convert_fusion.2 = bf16[11,2048]{1,0:T(8,128)(2,1)} fusion(bf16[256,2048]{0,1:T(8,128)(2,1)S(1)} %bitcast.77, bf16[11,2048]{1,0:T(8,128)(2,1)S(1)} %fusion.32, bf16[2048,256]{1,0:T(8,128)(2,1)} %all-gather.13.cloned.1.call-done, f32[11,256]{1,0:T(8,128)S(1)} %fusion.67), kind=kOutput, calls=%fused_computation.7 | convolution fusion | flops 23108096 | bytes 2198528 | tf_op jit(solution)/shard_map/dot_general | solution.py:100
  234.7 3.9 %all-to-all-done.1 = bf16[8,7,1024]{2,1,0:T(8,128)(2,1)S(1)} async-done(((bf16[8,7,1024]{2,1,0:T(8,128)(2,1)}), bf16[8,7,1024]{2,1,0:T(8,128)(2,1)S(1)}, u32[]{:S(2)}, u32[]{:S(2)}) %all-to-all-start.1) | async-done | bytes 114720 | tf_op jit(solution)/shard_map/all_to_all | solution.py:141
  239.0 6.3 %reduce-scatter.3.cloned.1.call-done = bf16[11,1024]{1,0:T(8,128)(2,1)} async-done(((bf16[11,2048]{1,0:T(8,128)(2,1)}), bf16[11,1024]{1,0:T(8,128)(2,1)}) %reduce-scatter.3.cloned.1.call-update) | async-done | bytes 22544 | tf_op jit(solution)/shard_map/reduce_scatter | solution.py:105
  245.3 1.4 add_convert_fusion
  (65 shorter events, 3.3 us)
Async XLA Ops:
  7.2 182.2 %copy-start = (bf16[1,256,2048]{2,1,0:T(8,128)(2,1)S(1)}, bf16[1,256,2048]{2,1,0:T(8,128)(2,1)}, u32[]{:S(2)}) copy-start(bf16[1,256,2048]{2,1,0:T(8,128)(2,1)} %param.32) | copy-start | bytes 3145732
  7.2 34.3 %all-gather.7.cloned.1.call-start = ((), (), s32[]{:S(2)}) async-start(), calls=%async_computation.4 | async-start | bytes 2359296 | tf_op jit(solution)/shard_map/all_gather | solution.py:64
  7.9 155.4 %all-gather.9.cloned.1.call-start = ((), (), s32[]{:S(2)}) async-start(), calls=%async_computation.5 | async-start | bytes 2359296 | tf_op jit(solution)/shard_map/all_gather | solution.py:83
  8.7 215.2 %all-gather.15.cloned.1.call-start = ((), (), s32[]{:S(2)}) async-start(), calls=%async_computation.10 | async-start | bytes 1179648 | tf_op jit(solution)/shard_map/all_gather | solution.py:98
  9.4 216.0 %all-gather.11.cloned.1.call-start = ((), (), s32[]{:S(2)}) async-start(), calls=%async_computation.6 | async-start | bytes 1179648 | tf_op jit(solution)/shard_map/all_gather | solution.py:90
  10.0 216.9 %reduce-scatter.5.cloned.1.call-start = ((), (), s32[]{:S(2)}) async-start(), calls=%async_computation.9 | async-start | bytes 344064 | tf_op jit(solution)/shard_map/reduce_scatter | solution.py:136
  11.0 13.0 %copy-start.9 = (s32[11]{0:T(128)S(1)}, s32[11]{0:T(128)}, u32[]{:S(2)}) copy-start(s32[11]{0:T(128)} %param.26) | copy-start | bytes 136
  11.0 13.1 %copy-start.10 = (f32[8]{0:T(128)S(1)}, f32[8]{0:T(128)}, u32[]{:S(2)}) copy-start(f32[8]{0:T(128)} %param.24) | copy-start | bytes 100
  11.0 13.2 %copy-start.7 = (s32[11,4]{0,1:T(4,128)S(1)}, s32[11,4]{0,1:T(4,128)}, u32[]{:S(2)}) copy-start(s32[11,4]{0,1:T(4,128)} %param.28) | copy-start | bytes 532
  11.0 30.5 %copy-start.1 = (bf16[11,2048]{1,0:T(8,128)(2,1)S(1)}, bf16[11,2048]{1,0:T(8,128)(2,1)}, u32[]{:S(2)}) copy-start(bf16[11,2048]{1,0:T(8,128)(2,1)} %param.18) | copy-start | bytes 135172
  11.0 30.5 %copy-start.3 = (f32[2048]{0:T(1024)S(1)}, f32[2048]{0:T(1024)}, u32[]{:S(2)}) copy-start(f32[2048]{0:T(1024)} %param.19) | copy-start | bytes 24580
  158.7 15.6 %copy-start.6 = (f32[2048]{0:T(1024)S(1)}, f32[2048]{0:T(1024)}, u32[]{:S(2)}) copy-start(f32[2048]{0:T(1024)} %param.20) | copy-start | bytes 24580
  158.7 28.7 %copy-start.2 = (bf16[1,2048,256]{2,1,0:T(8,128)(2,1)S(1)}, bf16[1,2048,256]{2,1,0:T(8,128)(2,1)}, u32[]{:S(2)}) copy-start(bf16[1,2048,256]{2,1,0:T(8,128)(2,1)} %param.31) | copy-start | bytes 3145732
  163.2 27.8 %copy-start.8 = (f32[11,4]{0,1:T(4,128)S(1)}, f32[11,4]{0,1:T(4,128)}, u32[]{:S(2)}) copy-start(f32[11,4]{0,1:T(4,128)} %param.29) | copy-start | bytes 532
  163.2 27.9 %copy-start.4 = (bf16[256,128]{1,0:T(8,128)(2,1)S(1)}, bf16[256,128]{1,0:T(8,128)(2,1)}, u32[]{:S(2)}) copy-start(bf16[256,128]{1,0:T(8,128)(2,1)} %param.22) | copy-start | bytes 196612
  163.2 43.1 %copy-start.5 = (bf16[256,128]{1,0:T(8,128)(2,1)S(1)}, bf16[256,128]{1,0:T(8,128)(2,1)}, u32[]{:S(2)}) copy-start(bf16[256,128]{1,0:T(8,128)(2,1)} %param.23) | copy-start | bytes 196612
  190.4 41.6 %all-gather.13.cloned.1.call-start = ((), (), s32[]{:S(2)}) async-start(), calls=%async_computation.7 | async-start | bytes 1179648 | tf_op jit(solution)/shard_map/all_gather | solution.py:91
  228.5 10.1 %all-to-all-start.1 = ((bf16[8,7,1024]{2,1,0:T(8,128)(2,1)}), bf16[8,7,1024]{2,1,0:T(8,128)(2,1)S(1)}, u32[]{:S(2)}, u32[]{:S(2)}) async-start(bf16[8,7,1024]{2,1,0:T(8,128)(2,1)} %copy.46), calls=%async_computation.3 | async-start | bytes 262144 | tf_op jit(solution)/shard_map/all_to_all | solution.py:141
  231.9 13.5 %reduce-scatter.3.cloned.1.call-start = ((), (), s32[]{:S(2)}) async-start(), calls=%async_computation.8 | async-start | bytes 98304 | tf_op jit(solution)/shard_map/reduce_scatter | solution.py:105
Sparse Core Ops, SparseCore 0:
  9.6 31.8 all-gather.6
  43.1 29.9 all-gather.8
  74.7 21.2 all-gather.14
  97.5 22.0 all-gather.10
  190.5 9.3 reduce-scatter.4
  201.3 24.5 all-gather.12
  234.9 10.4 reduce-scatter.2
